TPU v7x, 32 devices: a whole 2x2x4 slice. The times are simulated.
32 devices in a mesh: sp: 4 (over z), fs: 4 (over y, x), tp: 2 (over core).
Axes of the slice: x: 2, y: 2, z: 4, core: 2. Of those that a mesh axis runs over, the one named last changes fastest.
Arguments:
- tokens: bfloat16 [4, 1024, 2048], P('fs', 'sp'), may hold values from -6 to 6
- norm_gain: float32 [2048], replicated, may hold values from 0.1 to 1.9
- query_weight: bfloat16 [2048, 1024], P(('sp', 'fs'), 'tp'), may hold values from -0.125 to 0.125
- key_weight: bfloat16 [2048, 1024], P(('sp', 'fs'), 'tp'), may hold values from -0.125 to 0.125
- value_weight: bfloat16 [2048, 1024], P(('sp', 'fs'), 'tp'), may hold values from -0.125 to 0.125
- outgate_weight: bfloat16 [2048, 1024], P(('sp', 'fs'), 'tp'), may hold values from -0.125 to 0.125
- gate_weight: bfloat16 [4, 8, 2048], P(None, 'tp'), may hold values from -0.125 to 0.125
- gate_bias: float32 [4, 8], P(None, 'tp'), may hold values from -1 to 100
- decay_extra: float32 [4, 2, 8, 1024], P('fs', None, 'tp', 'sp'), may hold values from -0.75 to 0
- init_memory: float32 [4, 2, 8, 128, 128], P('fs', None, 'tp'), may hold values from -48 to 48
- init_normalizer: float32 [4, 2, 8, 128], P('fs', None, 'tp'), may hold values from -48 to 48
- head_gain: float32 [8, 128], P('tp'), may hold values from 0.1 to 1.9
- pool_weight: bfloat16 [2048, 2048], P(('sp', 'fs'), 'tp'), may hold values from -0.125 to 0.125
- mem_out_weight: bfloat16 [2048, 1024], P(('sp', 'fs'), 'tp'), may hold values from -0.1875 to 0.1875
- pool_out_weight: bfloat16 [2048, 2048], P(('sp', 'fs'), 'tp'), may hold values from -0.125 to 0.125
Outputs:
- mixed: bfloat16 [4, 1024, 2048], P('fs', ('sp', 'tp'))
All inputs are finite; a program needn't handle non-finite values.
Results may differ from a plain program's by a relative error of at most 0.014.
Values may be sent and summed in bfloat16 or wider, within the bound.
A program may use at most 64 MiB of HBM per device.

v0:
```python
import math
import jax
import jax.numpy as jnp
from jax import lax
from jax.sharding import PartitionSpec as P

HALO = 8
norm_eps = 1e-06
exact_mode = lax.Precision.HIGHEST


def carried_in(x, axis, combine, identity, reverse):
    length, position = (lax.axis_size(axis), lax.axis_index(axis))
    everything = jax.tree.map(lambda part: lax.all_gather(part, axis), x)
    start = jax.tree.map(
        lambda part, zero: jnp.broadcast_to(jnp.asarray(zero, part.dtype), part.shape), x, identity
    )

    def lap(k, before):
        at = length - 1 - k if reverse else k
        reached = at > position if reverse else at < position
        new = combine(before, jax.tree.map(lambda part: part[at], everything))
        return jax.tree.map(lambda a, b: jnp.where(reached, a, b), new, before)

    return lax.fori_loop(0, length, lap, start)


def padded_2(block, sides, width):
    for axis, dim in sides:
        count = lax.axis_size(axis)
        forward = [(i, i + 1) for i in range(count - 1)]
        backward = [(target, source) for source, target in forward]
        low = lax.ppermute(
            lax.slice_in_dim(block, block.shape[dim] - width, None, axis=dim), axis, forward
        )
        high = lax.ppermute(lax.slice_in_dim(block, 0, width, axis=dim), axis, backward)
        block = jnp.concatenate([low, block, high], axis=dim)
    return block


def block_output(
    query_rows, key_rows, value_rows, input_gate, log_forget, memory, normalizer, stabilizer
):
    block_len = query_rows.shape[1]
    key_scale = key_rows.shape[-1] ** (-0.5)
    lower_mask = jnp.tril(jnp.ones((block_len, block_len), dtype=bool))
    summed = jnp.cumsum(log_forget, axis=-1)
    log_decay = jnp.where(
        lower_mask, summed[:, :, None] - summed[:, None, :] + input_gate[:, None, :], -jnp.inf
    )
    log_carry = stabilizer[:, None] + summed
    running_max = jnp.maximum(log_carry, jnp.max(log_decay, axis=-1))
    scores = (
        jnp.einsum("btd,bsd->bts", query_rows, key_rows, preferred_element_type=jnp.float32)
        * key_scale
    )
    inner_weight = jnp.exp(log_decay - running_max[:, :, None]) * scores
    weight_rounded = inner_weight.astype(jnp.bfloat16)
    carry_weight = jnp.exp(log_carry - running_max)
    query_wide = query_rows.astype(jnp.float32)
    numerator = carry_weight[:, :, None] * jnp.einsum(
        "bed,btd->bte", memory, query_wide, precision=exact_mode
    )
    numerator = numerator + jnp.einsum(
        "bts,bse->bte", weight_rounded, value_rows, preferred_element_type=jnp.float32
    )
    denominator = carry_weight * jnp.einsum(
        "bd,btd->bt", normalizer, query_wide, precision=exact_mode
    )
    denominator = denominator + jnp.sum(inner_weight, axis=-1)
    return numerator / jnp.maximum(jnp.abs(denominator), jnp.exp(-running_max))[:, :, None]


def block_summary(key_rows, value_rows, input_gate, log_forget):
    key_wide = key_rows.astype(jnp.float32) * key_rows.shape[-1] ** (-0.5)
    summed = jnp.cumsum(log_forget, axis=-1)
    forget_total = summed[:, -1]
    log_weight = forget_total[:, None] - summed + input_gate
    running_max = jnp.max(log_weight, axis=-1)
    weights = jnp.exp(log_weight - running_max[:, None])
    memory = jnp.einsum(
        "bse,bsd->bed",
        weights[:, :, None] * value_rows.astype(jnp.float32),
        key_wide,
        precision=exact_mode,
    )
    normalizer = jnp.einsum("bs,bsd->bd", weights, key_wide, precision=exact_mode)
    return (memory, normalizer, running_max, forget_total)


def combine(earlier, latter):
    early_memory, early_norm, early_max, early_total = earlier
    late_memory, late_norm, late_max, late_total = latter
    joint_max = jnp.maximum(early_max + late_total, late_max)
    early_scale = jnp.exp(early_max + late_total - joint_max)
    late_scale = jnp.exp(late_max - joint_max)
    memory = early_scale[:, None, None] * early_memory + late_scale[:, None, None] * late_memory
    normalizer = early_scale[:, None] * early_norm + late_scale[:, None] * late_norm
    return (memory, normalizer, joint_max, early_total + late_total)


def span_sweep(
    query_rows, key_rows, value_rows, input_gate, log_forget, memory, normalizer, stabilizer, span
):
    block_count = query_rows.shape[1] // span

    def to_blocks(array):
        shaped = array.reshape((array.shape[0], block_count, span) + array.shape[2:])
        return jnp.moveaxis(shaped, 1, 0)

    def advance(carried, pieces):
        query_blk, key_blk, value_blk, gate_blk, forget_blk = pieces
        result = block_output(
            query_blk, key_blk, value_blk, gate_blk, forget_blk, carried[0], carried[1], carried[2]
        )
        return (combine(carried, block_summary(key_blk, value_blk, gate_blk, forget_blk)), result)

    initial = (memory, normalizer, stabilizer, jnp.zeros_like(stabilizer))
    ignored, outputs = lax.scan(
        advance,
        initial,
        tuple(
            (
                to_blocks(array)
                for array in (query_rows, key_rows, value_rows, input_gate, log_forget)
            )
        ),
    )
    return jnp.moveaxis(outputs, 0, 1).reshape(query_rows.shape[:2] + (value_rows.shape[2],))


def reverse_time(array):
    return jnp.flip(array, axis=1)


def to_heads(matrix, head_count):
    shaped = matrix.reshape(matrix.shape[0], head_count, matrix.shape[1] // head_count)
    return shaped.transpose(1, 0, 2)


def pool_window(padded, positions, channels, seq_len, group_size):
    row_count = positions.shape[0]
    group_index = channels // group_size
    reach_left = jnp.left_shift(jnp.ones_like(group_index), group_index)
    reach_right = reach_left - 1
    window_sum = jnp.zeros((row_count, channels.shape[0]), jnp.float32)
    for offset in range(-HALO, HALO):
        inside = ((offset >= -reach_left) & (offset <= reach_right)).astype(jnp.float32)
        window_sum = window_sum + inside * padded[HALO + offset : HALO + offset + row_count]
    first_pos = jnp.maximum(positions[:, None] - reach_left[None, :], 0)
    last_pos = jnp.minimum(positions[:, None] + reach_right[None, :], seq_len - 1)
    counted = (last_pos - first_pos + 1).astype(jnp.float32)
    centre = padded[HALO : HALO + row_count]
    return (window_sum / counted - centre).astype(jnp.bfloat16)


def per_device(
    tokens,
    norm_gain,
    query_weight,
    key_weight,
    value_weight,
    outgate_weight,
    gate_weight,
    gate_bias,
    decay_extra,
    init_memory,
    init_normalizer,
    head_gain,
    pool_weight,
    mem_out_weight,
    pool_out_weight,
):
    block_len = tokens.shape[1]
    model_width = tokens.shape[2]
    head_count, head_width = head_gain.shape
    span = math.gcd(block_len, 256)
    flattened = tokens[0].astype(jnp.float32)
    normed = (
        flattened
        * lax.rsqrt(jnp.mean(flattened * flattened, axis=-1, keepdims=True) + norm_eps)
        * norm_gain
    ).astype(jnp.bfloat16)
    zero_start = tuple(
        (
            jnp.zeros((block_len, weight.shape[1]), jnp.float32)
            for weight in (query_weight, key_weight, value_weight, outgate_weight, pool_weight)
        )
    )
    zero_start = zero_start + (
        jnp.zeros((model_width, mem_out_weight.shape[1]), jnp.bfloat16),
        jnp.zeros((model_width, pool_out_weight.shape[1]), jnp.bfloat16),
    )
    line_query, line_key, line_value, line_outgate, line_pool, line_mem_out, line_pool_out = (
        lax.all_gather(query_weight, "fs", axis=0, tiled=True),
        lax.all_gather(key_weight, "fs", axis=0, tiled=True),
        lax.all_gather(value_weight, "fs", axis=0, tiled=True),
        lax.all_gather(outgate_weight, "fs", axis=0, tiled=True),
        lax.all_gather(pool_weight, "fs", axis=0, tiled=True),
        lax.all_gather(mem_out_weight, "fs", axis=0, tiled=True),
        lax.all_gather(pool_out_weight, "fs", axis=0, tiled=True),
    )
    pieces = (
        lax.all_gather(line_query, "sp", axis=0, tiled=True),
        lax.all_gather(line_key, "sp", axis=0, tiled=True),
        lax.all_gather(line_value, "sp", axis=0, tiled=True),
        lax.all_gather(line_outgate, "sp", axis=0, tiled=True),
        lax.all_gather(line_pool, "sp", axis=0, tiled=True),
        lax.all_gather(line_mem_out, "sp", axis=0, tiled=True),
        lax.all_gather(line_pool_out, "sp", axis=0, tiled=True),
    )
    partial_sums = tuple(
        (
            jnp.dot(normed, weight_rows, preferred_element_type=jnp.float32)
            for weight_rows in pieces[:5]
        )
    )
    collected = tuple((weight_rows for weight_rows in pieces[5:]))
    folded = partial_sums + collected
    query_proj, key_proj, value_proj, outgate, pool_input = tuple(
        (running.astype(jnp.bfloat16) for running in folded[:5])
    )
    mem_weight_all = folded[5]
    pool_weight_all = folded[6]
    gate_pre = lax.dot_general(
        normed,
        gate_weight.reshape(4 * head_count, model_width),
        (((1,), (1,)), ((), ())),
        preferred_element_type=jnp.float32,
    ) + gate_bias.reshape(4 * head_count)
    gate_pre = gate_pre.reshape(block_len, 4, head_count).transpose(1, 2, 0)
    query_heads = to_heads(query_proj, head_count)
    key_heads = to_heads(key_proj, head_count)
    value_heads = to_heads(value_proj, head_count)
    forward_forget = jax.nn.log_sigmoid(gate_pre[1]) + decay_extra[0, 0]
    backward_forget = jax.nn.log_sigmoid(gate_pre[3]) + decay_extra[0, 1]
    zero_rows = jnp.zeros((head_count,), jnp.float32)
    identity = (
        jnp.zeros((head_count, head_width, head_width), jnp.float32),
        jnp.zeros((head_count, head_width), jnp.float32),
        jnp.full((head_count,), -1e30, jnp.float32),
        zero_rows,
    )
    front_memory, front_norm, front_max, front_total = block_summary(
        key_heads, value_heads, gate_pre[0], forward_forget
    )
    prefix = carried_in(
        (front_memory, front_norm, front_max, front_total), "sp", combine, identity, False
    )
    incoming = combine((init_memory[0, 0], init_normalizer[0, 0], zero_rows, zero_rows), prefix)
    forward_out = span_sweep(
        query_heads,
        key_heads,
        value_heads,
        gate_pre[0],
        forward_forget,
        incoming[0],
        incoming[1],
        incoming[2],
        span,
    )
    back_query = reverse_time(query_heads)
    back_key = reverse_time(key_heads)
    back_value = reverse_time(value_heads)
    back_gate = reverse_time(gate_pre[2])
    back_forget = reverse_time(backward_forget)
    rear_memory, rear_norm, rear_max, rear_total = block_summary(
        back_key, back_value, back_gate, back_forget
    )
    suffix = carried_in(
        (rear_memory, rear_norm, rear_max, rear_total), "sp", combine, identity, True
    )
    back_incoming = combine(
        (init_memory[0, 1], init_normalizer[0, 1], zero_rows, zero_rows), suffix
    )
    backward_out = reverse_time(
        span_sweep(
            back_query,
            back_key,
            back_value,
            back_gate,
            back_forget,
            back_incoming[0],
            back_incoming[1],
            back_incoming[2],
            span,
        )
    )
    summed_dirs = (forward_out + backward_out).transpose(1, 0, 2)
    normed_heads = (
        summed_dirs
        * lax.rsqrt(jnp.mean(summed_dirs * summed_dirs, axis=-1, keepdims=True) + norm_eps)
        * head_gain
    )
    out_gate = jax.nn.sigmoid(
        outgate.astype(jnp.float32).reshape(block_len, head_count, head_width)
    )
    memory_out = (
        (normed_heads * out_gate).astype(jnp.bfloat16).reshape(block_len, head_count * head_width)
    )
    padded = padded_2(pool_input, (("sp", 0),), HALO).astype(jnp.float32)
    feature_count = pool_input.shape[1]
    positions = lax.axis_index("sp") * block_len + jnp.arange(block_len, dtype=jnp.int32)
    channels = lax.axis_index("tp") * feature_count + jnp.arange(feature_count, dtype=jnp.int32)
    pool_out = pool_window(
        padded, positions, channels, block_len * lax.axis_size("sp"), model_width // 4
    )
    own_rows = block_len // lax.axis_size("tp")
    result = lax.dot_general(
        memory_out, mem_weight_all, (((1,), (1,)), ((), ())), preferred_element_type=jnp.float32
    )
    mixed = lax.psum_scatter(
        (
            result
            + lax.dot_general(
                pool_out,
                pool_weight_all,
                (((1,), (1,)), ((), ())),
                preferred_element_type=jnp.float32,
            )
        ).astype(jnp.bfloat16),
        "tp",
        scatter_dimension=0,
        tiled=True,
    )
    return mixed.reshape(1, own_rows, model_width)


def solution(mesh):
    placed = (
        P("fs", "sp", None),
        P(),
        P(("sp", "fs"), "tp"),
        P(("sp", "fs"), "tp"),
        P(("sp", "fs"), "tp"),
        P(("sp", "fs"), "tp"),
        P(None, "tp", None),
        P(None, "tp"),
        P("fs", None, "tp", "sp"),
        P("fs", None, "tp", None, None),
        P("fs", None, "tp", None),
        P("tp", None),
        P(("sp", "fs"), "tp"),
        P(("sp", "fs"), "tp"),
        P(("sp", "fs"), "tp"),
    )
    return jax.shard_map(
        per_device,
        mesh=mesh,
        in_specs=placed,
        out_specs=P("fs", ("sp", "tp"), None),
        check_vma=False,
    )
```

profile of v0, /device:TPU:0, one launch (start us, length us, event | category | flops | bytes accessed | tf_op | source)
XLA Modules:
  0.0 544.0 jit_solution(11762868126986876266)
XLA Ops:
  6.5 13.3 %all_gather.89 = bf16[512,512]{1,0:T(8,128)(2,1)} all-gather(bf16[128,512]{1,0:T(8,128)(2,1)} %param.22), channel_id=1, replica_groups=mesh['sp'=4,'fs'=4,'tp'=2] {'fs'}, dimensions={0}, use_global_device_ids=true | all-gather | bytes 655360 | tf_op jit(solution)/shard_map/all_gather | solution.py:196
  19.9 11.6 %all_gather.87 = bf16[512,512]{1,0:T(8,128)(2,1)} all-gather(bf16[128,512]{1,0:T(8,128)(2,1)} %param.23), channel_id=1, replica_groups=mesh['sp'=4,'fs'=4,'tp'=2] {'fs'}, dimensions={0}, use_global_device_ids=true | all-gather | bytes 655360 | tf_op jit(solution)/shard_map/all_gather | solution.py:197
  32.9 10.5 %all_gather.95 = bf16[512,512]{1,0:T(8,128)(2,1)} all-gather(bf16[128,512]{1,0:T(8,128)(2,1)S(1)} %copy-done.3), channel_id=1, replica_groups=mesh['sp'=4,'fs'=4,'tp'=2] {'fs'}, dimensions={0}, use_global_device_ids=true | all-gather | bytes 655360 | tf_op jit(solution)/shard_map/all_gather | solution.py:195
  43.5 10.5 %all_gather.104 = bf16[512,512]{1,0:T(8,128)(2,1)} all-gather(bf16[128,512]{1,0:T(8,128)(2,1)S(1)} %copy-done.4), channel_id=1, replica_groups=mesh['sp'=4,'fs'=4,'tp'=2] {'fs'}, dimensions={0}, use_global_device_ids=true | all-gather | bytes 655360 | tf_op jit(solution)/shard_map/all_gather | solution.py:198
  55.1 1.2 reduce-window.24
  57.2 8.7 %all-gather.24.cloned.1.call-done = bf16[2048,512]{1,0:T(8,128)(2,1)} async-done(((bf16[512,512]{1,0:T(8,128)(2,1)}), bf16[2048,512]{1,0:T(8,128)(2,1)}) %all-gather.24.cloned.1.call-update) | async-done | bytes 2097168 | tf_op jit(solution)/shard_map/all_gather | solution.py:205
  65.9 2.3 fusion.36
  68.3 43.7 %all-gather.22.cloned.1.call-done = bf16[2048,512]{1,0:T(8,128)(2,1)} async-done(((bf16[512,512]{1,0:T(8,128)(2,1)}), bf16[2048,512]{1,0:T(8,128)(2,1)}) %all-gather.22.cloned.1.call-update) | async-done | bytes 2097168 | tf_op jit(solution)/shard_map/all_gather | solution.py:206
  112.0 2.3 fusion.35
  114.3 1.9 fusion.71
  116.5 1.2 reduce-window.26
  119.5 1.9 fusion.65
  121.5 17.7 %all-gather.32.cloned.1.call-done = bf16[512,1024]{1,0:T(8,128)(2,1)} async-done(((bf16[128,1024]{1,0:T(8,128)(2,1)}), bf16[512,1024]{1,0:T(8,128)(2,1)}) %all-gather.32.cloned.1.call-update) | async-done | bytes 1048592 | tf_op jit(solution)/shard_map/all_gather | solution.py:199
  139.3 28.2 %all-gather.36.cloned.1.call-done = bf16[512,1024]{1,0:T(8,128)(2,1)} async-done(((bf16[128,1024]{1,0:T(8,128)(2,1)}), bf16[512,1024]{1,0:T(8,128)(2,1)}) %all-gather.36.cloned.1.call-update) | async-done | bytes 1048592 | tf_op jit(solution)/shard_map/all_gather | solution.py:201
  167.5 10.6 %all_gather.106 = bf16[512,512]{1,0:T(8,128)(2,1)} all-gather(bf16[128,512]{1,0:T(8,128)(2,1)S(1)} %copy-done.5), channel_id=1, replica_groups=mesh['sp'=4,'fs'=4,'tp'=2] {'fs'}, dimensions={0}, use_global_device_ids=true | all-gather | bytes 655360 | tf_op jit(solution)/shard_map/all_gather | solution.py:200
  185.9 12.3 %all-reduce.4 = (f32[16]{0:T(128)S(1)}, f32[16]{0:T(128)S(1)}, f32[16]{0:T(128)S(1)}, f32[16]{0:T(128)S(1)}) all-reduce(f32[16]{0:T(128)S(1)} %dynamic-update-slice.2, f32[16]{0:T(128)S(1)} %dynamic-update-slice.3, f32[16]{0:T(128)S(1)} %dynamic-update-slice, f32[16]{0:T(128)S(1)} %dynamic-update-slice.1), channel_id=6, replica_groups=mesh['sp'=4,'fs'=4,'tp'=2] {'sp'}, use_global_device_ids=true, to_apply=%add.2 | all-reduce | flops 64 | bytes 512
  201.4 12.5 %all-gather.8 = f32[4,4,128]{2,1,0:T(4,128)S(1)} all-gather(f32[1,4,128]{2,1,0:T(4,128)S(1)} %bitcast.306), channel_id=5, replica_groups=mesh['sp'=4,'fs'=4,'tp'=2] {'sp'}, dimensions={0}, use_global_device_ids=true | all-gather | bytes 10240 | tf_op jit(solution)/shard_map/all_gather | solution.py:14
  214.2 12.1 %all-gather.9 = f32[4,4,128]{2,1,0:T(4,128)S(1)} all-gather(f32[1,4,128]{2,1,0:T(4,128)S(1)} %bitcast.302), channel_id=9, replica_groups=mesh['sp'=4,'fs'=4,'tp'=2] {'sp'}, dimensions={0}, use_global_device_ids=true | all-gather | bytes 10240 | tf_op jit(solution)/shard_map/all_gather | solution.py:14
  226.4 2.3 fusion.37
  229.1 31.8 %all-gather.28.cloned.1.call-done = bf16[2048,512]{1,0:T(8,128)(2,1)} async-done(((bf16[512,512]{1,0:T(8,128)(2,1)}), bf16[2048,512]{1,0:T(8,128)(2,1)}) %all-gather.28.cloned.1.call-update) | async-done | bytes 2097168 | tf_op jit(solution)/shard_map/all_gather | solution.py:207
  260.9 3.2 fusion.34
  264.1 1.2 copy.60
  265.4 23.9 %all-gather.40.cloned.1.call-done = f32[16,128,128]{2,1,0:T(8,128)} async-done(((f32[4,128,128]{2,1,0:T(8,128)}), f32[16,128,128]{2,1,0:T(8,128)}) %all-gather.40.cloned.1.call-update) | async-done | bytes 1048592 | tf_op jit(solution)/shard_map/all_gather | solution.py:14
  289.3 7.4 %while.12 = (s32[]{:T(128)}, f32[4,128,128]{2,1,0:T(8,128)S(1)}, f32[4,128]{1,0:T(4,128)S(1)}, f32[4]{0:T(128)S(1)}, f32[4]{0:T(128)S(1)}, /*index=5*/s32[]{:T(1...) while((s32[]{:T(128)}, f32[4,128,128]{2,1,0:T(8,128)S(1)}, ...), condition=%wide.region_5.6_spmd.clone, body=%wide.region_4.5_spmd.clone.sunk | while | flops 330284 | bytes 792973 | solution.py:25
  290.0 1.1 fusion.157
  291.8 1.1 fusion.157
  293.7 1.1 fusion.157
  295.5 1.1 fusion.157
  297.8 2.3 fusion.133
  300.1 18.2 %all-gather.42.cloned.1.call-done = f32[16,128,128]{2,1,0:T(8,128)} async-done(((f32[4,128,128]{2,1,0:T(8,128)}), f32[16,128,128]{2,1,0:T(8,128)}) %all-gather.42.cloned.1.call-update) | async-done | bytes 1048592 | tf_op jit(solution)/shard_map/all_gather | solution.py:14
  318.3 7.5 %while.13 = (s32[]{:T(128)}, f32[4,128,128]{2,1,0:T(8,128)S(1)}, f32[4,128]{1,0:T(4,128)S(1)}, f32[4]{0:T(128)S(1)}, f32[4]{0:T(128)S(1)}, /*index=5*/s32[]{:T(1...) while((s32[]{:T(128)}, f32[4,128,128]{2,1,0:T(8,128)S(1)}, ...), condition=%wide.region_12.13_spmd.clone, body=%wide.region_11.12_spmd.clone.sunk | while | flops 330288 | bytes 793035 | solution.py:25
  319.0 1.1 fusion.159
  320.9 1.1 fusion.159
  322.7 1.1 fusion.159
  324.6 1.1 fusion.159
  327.7 1.2 fusion.25
  329.0 5.0 rev.26
  334.4 1.7 multiply_reduce_fusion
  336.1 63.9 %all-gather.34.cloned.1.call-done = bf16[2048,1024]{1,0:T(8,128)(2,1)} async-done(((bf16[512,1024]{1,0:T(8,128)(2,1)}), bf16[2048,1024]{1,0:T(8,128)(2,1)}) %all-gather.34.cloned.1.call-update) | async-done | bytes 4194320 | tf_op jit(solution)/shard_map/all_gather | solution.py:208
  400.0 3.5 convolution_convert_fusion
  403.7 1.3 collective-permute-start
  405.0 1.3 collective-permute-start.1
  406.4 4.2 collective-permute-done.1
  410.8 69.9 %all-gather.38.cloned.1.call-done = bf16[2048,1024]{1,0:T(8,128)(2,1)} async-done(((bf16[512,1024]{1,0:T(8,128)(2,1)}), bf16[2048,1024]{1,0:T(8,128)(2,1)}) %all-gather.38.cloned.1.call-update) | async-done | bytes 4194320 | tf_op jit(solution)/shard_map/all_gather | solution.py:210
  480.8 5.3 fusion.74
  486.1 40.3 %all-gather.30.cloned.1.call-done = bf16[2048,512]{1,0:T(8,128)(2,1)} async-done(((bf16[512,512]{1,0:T(8,128)(2,1)}), bf16[2048,512]{1,0:T(8,128)(2,1)}) %all-gather.30.cloned.1.call-update) | async-done | bytes 2097168 | tf_op jit(solution)/shard_map/all_gather | solution.py:209
  526.4 3.4 fusion.16
  529.8 7.3 %reduce-scatter.2.cloned.1.call-done = bf16[128,2048]{1,0:T(8,128)(2,1)} async-done(((bf16[256,2048]{1,0:T(8,128)(2,1)}), bf16[128,2048]{1,0:T(8,128)(2,1)}) %reduce-scatter.2.cloned.1.call-update) | async-done | bytes 524304 | tf_op jit(solution)/shard_map/reduce_scatter | solution.py:312
  (220 shorter events, 26.4 us)
Async XLA Ops:
  6.5 26.4 %copy-start.3 = (bf16[128,512]{1,0:T(8,128)(2,1)S(1)}, bf16[128,512]{1,0:T(8,128)(2,1)}, u32[]{:S(2)}) copy-start(bf16[128,512]{1,0:T(8,128)(2,1)} %param.21) | copy-start | bytes 393220
  6.5 37.0 %copy-start.4 = (bf16[128,512]{1,0:T(8,128)(2,1)S(1)}, bf16[128,512]{1,0:T(8,128)(2,1)}, u32[]{:S(2)}) copy-start(bf16[128,512]{1,0:T(8,128)(2,1)} %param.24) | copy-start | bytes 393220
  6.5 59.4 %all-gather.24.cloned.1.call-start = ((), (), s32[]{:S(2)}) async-start(), calls=%async_computation.2 | async-start | bytes 2621440 | tf_op jit(solution)/shard_map/all_gather | solution.py:205
  19.9 34.3 %copy-start.6 = (bf16[4,4,2048]{2,1,0:T(4,128)(2,1)S(1)}, bf16[4,4,2048]{2,1,0:T(4,128)(2,1)}, u32[]{:S(2)}) copy-start(bf16[4,4,2048]{2,1,0:T(4,128)(2,1)} %param.25) | copy-start | bytes 196612
  19.9 34.3 %copy-start.28 = (f32[4,4]{1,0:T(4,128)S(1)}, f32[4,4]{1,0:T(4,128)}, u32[]{:S(2)}) copy-start(f32[4,4]{1,0:T(4,128)} %param.26) | copy-start | bytes 196
  19.9 34.4 %copy-start = (bf16[1,256,2048]{2,1,0:T(8,128)(2,1)S(1)}, bf16[1,256,2048]{2,1,0:T(8,128)(2,1)}, u32[]{:S(2)}) copy-start(bf16[1,256,2048]{2,1,0:T(8,128)(2,1)} %param.19) | copy-start | bytes 3145732
  19.9 92.1 %all-gather.22.cloned.1.call-start = ((), (), s32[]{:S(2)}) async-start(), calls=%async_computation.1 | async-start | bytes 2621440 | tf_op jit(solution)/shard_map/all_gather | solution.py:206
  31.5 23.0 %copy-start.34 = (f32[2048]{0:T(1024)S(1)}, f32[2048]{0:T(1024)}, u32[]{:S(2)}) copy-start(f32[2048]{0:T(1024)} %param.20) | copy-start | bytes 24580
  31.5 107.7 %all-gather.32.cloned.1.call-start = ((), (), s32[]{:S(2)}) async-start(), calls=%async_computation.6 | async-start | bytes 1310720 | tf_op jit(solution)/shard_map/all_gather | solution.py:199
  32.3 135.2 %all-gather.36.cloned.1.call-start = ((), (), s32[]{:S(2)}) async-start(), calls=%async_computation.8 | async-start | bytes 1310720 | tf_op jit(solution)/shard_map/all_gather | solution.py:201
  32.8 193.5 %all-gather.26.cloned.1.call-start = ((), (), s32[]{:S(2)}) async-start(), calls=%async_computation.3 | async-start | bytes 2621440 | tf_op jit(solution)/shard_map/all_gather | solution.py:204
  43.4 11.7 %slice-start = ((f32[1,2,4,256]{3,2,1,0:T(4,128)}), f32[1,1,4,256]{3,2,1,0:T(4,128)S(1)}, s32[]{:S(2)}) async-start(f32[1,2,4,256]{3,2,1,0:T(4,128)} %param.27), calls=%async_computation.13 | async-start | bytes 8192 | tf_op jit(solution)/shard_map/slice | solution.py:235
  43.4 13.7 %copy-start.7 = (f32[1,2,4,256]{3,2,1,0:T(4,128)S(1)}, f32[1,2,4,256]{3,2,1,0:T(4,128)}, u32[]{:S(2)}) copy-start(f32[1,2,4,256]{3,2,1,0:T(4,128)} %param.27) | copy-start | bytes 24580
  43.5 217.5 %all-gather.28.cloned.1.call-start = ((), (), s32[]{:S(2)}) async-start(), calls=%async_computation.4 | async-start | bytes 2621440 | tf_op jit(solution)/shard_map/all_gather | solution.py:207
  54.1 235.2 %all-gather.40.cloned.1.call-start = ((), (), s32[]{:S(2)}) async-start(), calls=%async_computation.11 | async-start | bytes 1310720 | tf_op jit(solution)/shard_map/all_gather | solution.py:14
  54.6 206.3 %copy-start.30 = (f32[256]{0:T(256)}, f32[256]{0:T(256)S(1)}, u32[]{:S(2)}) copy-start(f32[256]{0:T(256)S(1)} %add_rsqrt_fusion.1) | copy-start | bytes 3076
  68.3 132.7 %copy-start.2 = (bf16[32,4,8,128]{3,2,1,0:T(8,128)(2,1)}, bf16[32,4,8,128]{3,2,1,0:T(8,128)(2,1)S(1)}, u32[]{:S(2)}) copy-start(bf16[32,4,8,128]{3,2,1,0:T(8,128)(2,1)S(1)} %fusion.36) | copy-start | bytes 786436
  116.2 202.0 %all-gather.42.cloned.1.call-start = ((), (), s32[]{:S(2)}) async-start(), calls=%async_computation.12 | async-start | bytes 1310720 | tf_op jit(solution)/shard_map/all_gather | solution.py:14
  118.9 48.7 %copy-start.5 = (bf16[128,512]{1,0:T(8,128)(2,1)S(1)}, bf16[128,512]{1,0:T(8,128)(2,1)}, u32[]{:S(2)}) copy-start(bf16[128,512]{1,0:T(8,128)(2,1)} %param.32) | copy-start | bytes 393220
  119.5 64.3 %copy-start.37 = (u32[32]{0:T(128)S(1)}, u32[32]{0:T(128)}, u32[]{:S(2)}) copy-start(u32[32]{0:T(128)} %constant.215) | copy-start | bytes 388
  121.4 278.6 %all-gather.34.cloned.1.call-start = ((), (), s32[]{:S(2)}) async-start(), calls=%async_computation.7 | async-start | bytes 5242880 | tf_op jit(solution)/shard_map/all_gather | solution.py:208
  139.2 341.4 %all-gather.38.cloned.1.call-start = ((), (), s32[]{:S(2)}) async-start(), calls=%async_computation.9 | async-start | bytes 5242880 | tf_op jit(solution)/shard_map/all_gather | solution.py:210
  167.5 358.9 %all-gather.30.cloned.1.call-start = ((), (), s32[]{:S(2)}) async-start(), calls=%async_computation.5 | async-start | bytes 2621440 | tf_op jit(solution)/shard_map/all_gather | solution.py:209
  178.2 359.0 %reduce-scatter.2.cloned.1.call-start = ((), (), s32[]{:S(2)}) async-start(), calls=%async_computation.10 | async-start | bytes 1572864 | tf_op jit(solution)/shard_map/reduce_scatter | solution.py:312
  334.1 65.9 %copy-start.31 = (f32[256]{0:T(256)S(1)}, f32[256]{0:T(256)}, u32[]{:S(2)}) copy-start(f32[256]{0:T(256)} %copy-done.30) | copy-start | bytes 3076
  334.1 65.9 %copy-start.35 = (f32[2048]{0:T(1024)S(1)}, f32[2048]{0:T(1024)}, u32[]{:S(2)}) copy-start(f32[2048]{0:T(1024)} %param.20) | copy-start | bytes 24580
  336.1 70.2 %copy-start.27 = (f32[4,128]{1,0:T(4,128)S(1)}, f32[4,128]{1,0:T(4,128)}, u32[]{:S(2)}) copy-start(f32[4,128]{1,0:T(4,128)} %param.30) | copy-start | bytes 6148
  403.5 77.2 %copy-start.9 = (s32[1024]{0:T(1024)S(1)}, s32[1024]{0:T(1024)}, u32[]{:S(2)}) copy-start(s32[1024]{0:T(1024)} %get-tuple-element.635) | copy-start | bytes 12292
  403.5 77.2 %copy-start.10 = (s32[1024]{0:T(1024)S(1)}, s32[1024]{0:T(1024)}, u32[]{:S(2)}) copy-start(s32[1024]{0:T(1024)} %get-tuple-element.636) | copy-start | bytes 12292
  403.5 77.2 %copy-start.11 = (f32[1024]{0:T(1024)S(1)}, f32[1024]{0:T(1024)}, u32[]{:S(2)}) copy-start(f32[1024]{0:T(1024)} %get-tuple-element.637) | copy-start | bytes 12292
  403.5 77.2 %copy-start.12 = (f32[1024]{0:T(1024)S(1)}, f32[1024]{0:T(1024)}, u32[]{:S(2)}) copy-start(f32[1024]{0:T(1024)} %get-tuple-element.638) | copy-start | bytes 12292
  403.5 77.2 %copy-start.13 = (f32[1024]{0:T(1024)S(1)}, f32[1024]{0:T(1024)}, u32[]{:S(2)}) copy-start(f32[1024]{0:T(1024)} %get-tuple-element.639) | copy-start | bytes 12292
  403.5 77.2 %copy-start.14 = (f32[1024]{0:T(1024)S(1)}, f32[1024]{0:T(1024)}, u32[]{:S(2)}) copy-start(f32[1024]{0:T(1024)} %get-tuple-element.640) | copy-start | bytes 12292
  403.5 77.2 %copy-start.15 = (f32[1024]{0:T(1024)S(1)}, f32[1024]{0:T(1024)}, u32[]{:S(2)}) copy-start(f32[1024]{0:T(1024)} %get-tuple-element.641) | copy-start | bytes 12292
  403.5 77.2 %copy-start.16 = (f32[1024]{0:T(1024)S(1)}, f32[1024]{0:T(1024)}, u32[]{:S(2)}) copy-start(f32[1024]{0:T(1024)} %get-tuple-element.642) | copy-start | bytes 12292
  403.6 77.2 %copy-start.17 = (f32[1024]{0:T(1024)S(1)}, f32[1024]{0:T(1024)}, u32[]{:S(2)}) copy-start(f32[1024]{0:T(1024)} %get-tuple-element.643) | copy-start | bytes 12292
  403.6 77.2 %copy-start.18 = (f32[1024]{0:T(1024)S(1)}, f32[1024]{0:T(1024)}, u32[]{:S(2)}) copy-start(f32[1024]{0:T(1024)} %get-tuple-element.644) | copy-start | bytes 12292
  403.6 77.2 %copy-start.19 = (f32[1024]{0:T(1024)S(1)}, f32[1024]{0:T(1024)}, u32[]{:S(2)}) copy-start(f32[1024]{0:T(1024)} %get-tuple-element.645) | copy-start | bytes 12292
  403.6 77.2 %copy-start.20 = (f32[1024]{0:T(1024)S(1)}, f32[1024]{0:T(1024)}, u32[]{:S(2)}) copy-start(f32[1024]{0:T(1024)} %get-tuple-element.646) | copy-start | bytes 12292
  403.6 77.2 %copy-start.21 = (f32[1024]{0:T(1024)S(1)}, f32[1024]{0:T(1024)}, u32[]{:S(2)}) copy-start(f32[1024]{0:T(1024)} %get-tuple-element.647) | copy-start | bytes 12292
  403.6 77.2 %copy-start.22 = (f32[1024]{0:T(1024)S(1)}, f32[1024]{0:T(1024)}, u32[]{:S(2)}) copy-start(f32[1024]{0:T(1024)} %get-tuple-element.648) | copy-start | bytes 12292
  403.6 77.2 %copy-start.23 = (f32[1024]{0:T(1024)S(1)}, f32[1024]{0:T(1024)}, u32[]{:S(2)}) copy-start(f32[1024]{0:T(1024)} %get-tuple-element.649) | copy-start | bytes 12292
  403.6 77.2 %copy-start.24 = (f32[1024]{0:T(1024)S(1)}, f32[1024]{0:T(1024)}, u32[]{:S(2)}) copy-start(f32[1024]{0:T(1024)} %get-tuple-element.650) | copy-start | bytes 12292
  403.6 77.2 %copy-start.25 = (f32[1024]{0:T(1024)S(1)}, f32[1024]{0:T(1024)}, u32[]{:S(2)}) copy-start(f32[1024]{0:T(1024)} %get-tuple-element.651) | copy-start | bytes 12292
  403.6 77.2 %copy-start.26 = (f32[1024]{0:T(1024)S(1)}, f32[1024]{0:T(1024)}, u32[]{:S(2)}) copy-start(f32[1024]{0:T(1024)} %get-tuple-element.652) | copy-start | bytes 12292
  403.7 77.2 %copy-start.36 = (s32[256]{0:T(256)S(1)}, s32[256]{0:T(256)}, u32[]{:S(2)}) copy-start(s32[256]{0:T(256)} %iota_add_fusion.1) | copy-start | bytes 3076
  403.7 2.8 collective-permute-start
  405.0 5.7 %collective-permute-start.1 = (bf16[8,1024]{1,0:T(8,128)(2,1)S(1)}, bf16[8,1024]{1,0:T(8,128)(2,1)S(1)}, u32[]{:S(2)}, u32[]{:S(2)}) collective-permute-start(bf16[8,1024]{1,0:T(8,128)(2,1)S(1)} %get-tuple-element.621), channel_id=1, source_target_pairs={{8,0},{16,8},{24,16},{9,1},{17,9},{25,17},{10,2},{18,10},{26,18},{... | collective-permute-start | bytes 49160 | tf_op jit(solution)/shard_map/ppermute | solution.py:36
  (5 other events, 30.5 us)
Sparse Core Ops, SparseCore 0:
  20.0 45.9 all-gather.23
  67.5 44.4 all-gather.21
  113.8 25.3 all-gather.31
  140.9 26.4 all-gather.35
  168.9 46.0 all-gather.25
  216.4 44.4 all-gather.27
  262.5 26.7 all-gather.39
  290.9 27.3 all-gather.41
  319.8 80.1 all-gather.33
  401.4 79.2 all-gather.37
  482.2 44.1 all-gather.29
  529.9 7.1 reduce-scatter.1
where the time goes:
time: 545 us; the launch traced here: 544 us
  waiting for transfers between devices  359 us (66%)
  blocking collectives  93.4 us (17%)
  matrix products  34.2 us (6%)
  other arithmetic  26.8 us (5%)
  between operations  15 us (3%)
  local copies, waits for them, and re-layouts  12.1 us (2%)
    all_gather x1, waiting for transfers between devices, per_device(): lax.all_gather(line_pool_out, 'sp', axis=0, tiled=True)  69.9 us
    all_gather x1, waiting for transfers between devices, per_device(): lax.all_gather(line_pool, 'sp', axis=0, tiled=True)  63.9 us
    all_gather x1, waiting for transfers between devices, per_device(): lax.all_gather(line_value, 'sp', axis=0, tiled=True)  43.7 us
    all_gather x2, waiting for transfers between devices, carried_in(): everything = jax.tree.map(lambda part: lax.all_gather(part, axis), x)  42.1 us
    all_gather x1, waiting for transfers between devices, per_device(): lax.all_gather(line_mem_out, 'sp', axis=0, tiled=True)  40.3 us
    all_gather x1, waiting for transfers between devices, per_device(): lax.all_gather(line_outgate, 'sp', axis=0, tiled=True)  31.8 us
    all_gather x1, waiting for transfers between devices, per_device(): lax.all_gather(pool_out_weight, 'fs', axis=0, tiled=True)  28.2 us
    all_gather x2, blocking collectives, carried_in(): everything = jax.tree.map(lambda part: lax.all_gather(part, axis), x)  24.6 us
  transfers between devices with their start and end apart: 14, of which 12 were waited for; matrix products, arithmetic and copies ran while one was open for 13% of the time, Pallas kernels for 0%

commit v1 on v0

--- a/solution.py
+++ b/solution.py
@@ -7,6 +7,18 @@
 HALO = 8
 norm_eps = 1e-06
 exact_mode = lax.Precision.HIGHEST
+
+
+def doubled_up(shard, axis, dim):
+    ways, here, hop = (lax.axis_size(axis), lax.axis_index(axis), shard.shape[dim])
+    line, have = (shard, 1)
+    while have < ways:
+        line = jnp.concatenate(
+            [line, lax.ppermute(line, axis, [(d, (d - have) % ways) for d in range(ways)])],
+            axis=dim,
+        )
+        have = 2 * have
+    return jnp.roll(line, here * hop, axis=dim)
 
 
 def carried_in(x, axis, combine, identity, reverse):
@@ -204,7 +216,7 @@
         lax.all_gather(line_query, "sp", axis=0, tiled=True),
         lax.all_gather(line_key, "sp", axis=0, tiled=True),
         lax.all_gather(line_value, "sp", axis=0, tiled=True),
-        lax.all_gather(line_outgate, "sp", axis=0, tiled=True),
+        doubled_up(line_outgate, "sp", 0),
         lax.all_gather(line_pool, "sp", axis=0, tiled=True),
         lax.all_gather(line_mem_out, "sp", axis=0, tiled=True),
         lax.all_gather(line_pool_out, "sp", axis=0, tiled=True),

time: 545 us -> 544 us (level)
  waiting for transfers between devices: 359 us -> 317 us
  blocking collectives: 93.4 us -> 123 us
  starting transfers between devices: 3.03 us -> 9.97 us
    all_gather x2, waiting for transfers between devices: 42.1 us -> 0.02 us  [carried_in(): everything = jax.tree.map(lambda part: lax.all_gather(part, axis), x)]
    ppermute x0 -> x2, waiting for transfers between devices: none -> 35.3 us  [doubled_up(): lax.ppermute(line, axis, [(d, (d - have) % ways) for d in range(ways)])]
    all_gather x1 -> x0, waiting for transfers between devices: 31.8 us -> none  [per_device(): lax.all_gather(line_outgate, 'sp', axis=0, tiled=True)]
    unnamed x1, blocking collectives: 12.3 us -> 30.9 us
    all_gather x1, waiting for transfers between devices: 63.9 us -> 48.5 us  [per_device(): lax.all_gather(line_pool, 'sp', axis=0, tiled=True)]
    all_gather x2, blocking collectives: 24.6 us -> 37.6 us  [carried_in(): everything = jax.tree.map(lambda part: lax.all_gather(part, axis), x)]
    all_gather x1, waiting for transfers between devices: 8.72 us -> 20.2 us  [per_device(): lax.all_gather(line_key, 'sp', axis=0, tiled=True)]
    ppermute x0 -> x2, starting transfers between devices: none -> 6.96 us  [doubled_up(): lax.ppermute(line, axis, [(d, (d - have) % ways) for d in range(ways)])]
  transfers between devices with their start and end apart: 14 -> 15, of which waited for: 12 -> 11; matrix products, arithmetic and copies ran while one was open for 13% -> 13% of each run, Pallas kernels for 0% -> 0%
where the time goes in v1:
time: 544 us; the launch traced here: 542 us
  waiting for transfers between devices  317 us (58%)
  blocking collectives  123 us (23%)
  matrix products  32.8 us (6%)
  other arithmetic  28 us (5%)
  local copies, waits for them, and re-layouts  15.9 us (3%)
  between operations  14.7 us (3%)
  starting transfers between devices  9.97 us (2%)
    all_gather x1, waiting for transfers between devices, per_device(): lax.all_gather(line_pool_out, 'sp', axis=0, tiled=True)  70 us
    all_gather x1, waiting for transfers between devices, per_device(): lax.all_gather(line_pool, 'sp', axis=0, tiled=True)  48.5 us
    all_gather x1, waiting for transfers between devices, per_device(): lax.all_gather(line_value, 'sp', axis=0, tiled=True)  43.7 us
    all_gather x1, waiting for transfers between devices, per_device(): lax.all_gather(line_mem_out, 'sp', axis=0, tiled=True)  40.1 us
    all_gather x2, blocking collectives, carried_in(): everything = jax.tree.map(lambda part: lax.all_gather(part, axis), x)  37.6 us
    ppermute x2, waiting for transfers between devices, doubled_up(): lax.ppermute(line, axis, [(d, (d - have) % ways) for d in range(ways)])  35.3 us
    unnamed x1, blocking collectives  30.9 us
    all_gather x1, waiting for transfers between devices, per_device(): lax.all_gather(pool_out_weight, 'fs', axis=0, tiled=True)  28.2 us
  transfers between devices with their start and end apart: 15, of which 11 were waited for; matrix products, arithmetic and copies ran while one was open for 13% of the time, Pallas kernels for 0%

profile of v1, /device:TPU:0, one launch (start us, length us, event | category | flops | bytes accessed | tf_op | source)
XLA Modules:
  0.0 541.8 jit_solution(12215091409018974371)
XLA Ops:
  6.6 13.3 %all_gather.86 = bf16[512,512]{1,0:T(8,128)(2,1)} all-gather(bf16[128,512]{1,0:T(8,128)(2,1)} %param.22), channel_id=1, replica_groups=mesh['sp'=4,'fs'=4,'tp'=2] {'fs'}, dimensions={0}, use_global_device_ids=true | all-gather | bytes 655360 | tf_op jit(solution)/shard_map/all_gather | solution.py:208
  20.0 11.4 %all_gather.84 = bf16[512,512]{1,0:T(8,128)(2,1)} all-gather(bf16[128,512]{1,0:T(8,128)(2,1)} %param.23), channel_id=1, replica_groups=mesh['sp'=4,'fs'=4,'tp'=2] {'fs'}, dimensions={0}, use_global_device_ids=true | all-gather | bytes 655360 | tf_op jit(solution)/shard_map/all_gather | solution.py:209
  32.8 9.8 %all_gather.92 = bf16[512,512]{1,0:T(8,128)(2,1)} all-gather(bf16[128,512]{1,0:T(8,128)(2,1)S(1)} %copy-done.5), channel_id=1, replica_groups=mesh['sp'=4,'fs'=4,'tp'=2] {'fs'}, dimensions={0}, use_global_device_ids=true | all-gather | bytes 655360 | tf_op jit(solution)/shard_map/all_gather | solution.py:207
  43.7 1.2 reduce-window.24
  45.8 20.2 %all-gather.23.cloned.1.call-done = bf16[2048,512]{1,0:T(8,128)(2,1)} async-done(((bf16[512,512]{1,0:T(8,128)(2,1)}), bf16[2048,512]{1,0:T(8,128)(2,1)}) %all-gather.23.cloned.1.call-update) | async-done | bytes 2097168 | tf_op jit(solution)/shard_map/all_gather | solution.py:217
  66.0 2.3 fusion.51
  68.3 43.7 %all-gather.21.cloned.1.call-done = bf16[2048,512]{1,0:T(8,128)(2,1)} async-done(((bf16[512,512]{1,0:T(8,128)(2,1)}), bf16[2048,512]{1,0:T(8,128)(2,1)}) %all-gather.21.cloned.1.call-update) | async-done | bytes 2097168 | tf_op jit(solution)/shard_map/all_gather | solution.py:218
  112.1 2.3 fusion.50
  114.4 1.9 fusion.86
  116.6 1.2 reduce-window.26
  119.6 1.9 fusion.80
  121.5 17.8 %all-gather.29.cloned.1.call-done = bf16[512,1024]{1,0:T(8,128)(2,1)} async-done(((bf16[128,1024]{1,0:T(8,128)(2,1)}), bf16[512,1024]{1,0:T(8,128)(2,1)}) %all-gather.29.cloned.1.call-update) | async-done | bytes 1048592 | tf_op jit(solution)/shard_map/all_gather | solution.py:211
  139.4 28.2 %all-gather.33.cloned.1.call-done = bf16[512,1024]{1,0:T(8,128)(2,1)} async-done(((bf16[128,1024]{1,0:T(8,128)(2,1)}), bf16[512,1024]{1,0:T(8,128)(2,1)}) %all-gather.33.cloned.1.call-update) | async-done | bytes 1048592 | tf_op jit(solution)/shard_map/all_gather | solution.py:213
  167.6 10.1 %all_gather.101 = bf16[512,512]{1,0:T(8,128)(2,1)S(1)} all-gather(bf16[128,512]{1,0:T(8,128)(2,1)S(1)} %copy-done.6), channel_id=1, replica_groups=mesh['sp'=4,'fs'=4,'tp'=2] {'fs'}, dimensions={0}, use_global_device_ids=true | all-gather | bytes 655360 | tf_op jit(solution)/shard_map/all_gather | solution.py:210
  177.7 3.3 collective-permute-start
  181.0 10.5 %all_gather.102 = bf16[512,512]{1,0:T(8,128)(2,1)} all-gather(bf16[128,512]{1,0:T(8,128)(2,1)S(1)} %copy-done.7), channel_id=1, replica_groups=mesh['sp'=4,'fs'=4,'tp'=2] {'fs'}, dimensions={0}, use_global_device_ids=true | all-gather | bytes 655360 | tf_op jit(solution)/shard_map/all_gather | solution.py:212
  194.6 17.9 %collective-permute-done = bf16[512,512]{1,0:T(8,128)(2,1)S(1)} collective-permute-done((bf16[512,512]{1,0:T(8,128)(2,1)S(1)}, bf16[512,512]{1,0:T(8,128)(2,1)S(1)}, u32[]{:S(2)}, u32[]{:S(2)}) %collective-permute-start) | collective-permute-done | bytes 524320 | tf_op jit(solution)/shard_map/ppermute | solution.py:17
  212.5 1.1 pad_maximum_fusion
  213.6 3.6 collective-permute-start.1
  220.0 30.9 %all-reduce.4 = (f32[16]{0:T(128)S(1)}, f32[16]{0:T(128)S(1)}, f32[16]{0:T(128)S(1)}, f32[16]{0:T(128)S(1)}) all-reduce(f32[16]{0:T(128)S(1)} %dynamic-update-slice.2, f32[16]{0:T(128)S(1)} %dynamic-update-slice.3, f32[16]{0:T(128)S(1)} %dynamic-update-slice, f32[16]{0:T(128)S(1)} %dynamic-update-slice.1), channel_id=6, replica_groups=mesh['sp'=4,'fs'=4,'tp'=2] {'sp'}, use_global_device_ids=true, to_apply=%add.2 | all-reduce | flops 64 | bytes 512
  255.6 17.4 %collective-permute-done.1 = bf16[1024,512]{1,0:T(8,128)(2,1)S(1)} collective-permute-done((bf16[1024,512]{1,0:T(8,128)(2,1)}, bf16[1024,512]{1,0:T(8,128)(2,1)S(1)}, u32[]{:S(2)}, u32[]{:S(2)}) %collective-permute-start.1) | collective-permute-done | bytes 1048608 | tf_op jit(solution)/shard_map/ppermute | solution.py:17
  275.4 1.3 fusion.85
  276.8 25.1 %all-gather.8 = f32[4,4,128]{2,1,0:T(4,128)S(1)} all-gather(f32[1,4,128]{2,1,0:T(4,128)S(1)} %bitcast.305), channel_id=5, replica_groups=mesh['sp'=4,'fs'=4,'tp'=2] {'sp'}, dimensions={0}, use_global_device_ids=true | all-gather | bytes 10240 | tf_op jit(solution)/shard_map/all_gather | solution.py:26
  302.2 12.5 %all-gather.9 = f32[4,4,128]{2,1,0:T(4,128)S(1)} all-gather(f32[1,4,128]{2,1,0:T(4,128)S(1)} %bitcast.301), channel_id=9, replica_groups=mesh['sp'=4,'fs'=4,'tp'=2] {'sp'}, dimensions={0}, use_global_device_ids=true | all-gather | bytes 10240 | tf_op jit(solution)/shard_map/all_gather | solution.py:26
  314.7 2.4 fusion.52
  317.8 3.2 rev.25
  321.0 7.5 %while.12 = (s32[]{:T(128)}, f32[4,128,128]{2,1,0:T(8,128)S(1)}, f32[4,128]{1,0:T(4,128)S(1)}, f32[4]{0:T(128)S(1)}, f32[4]{0:T(128)S(1)}, /*index=5*/s32[]{:T(1...) while((s32[]{:T(128)}, f32[4,128,128]{2,1,0:T(8,128)S(1)}, ...), condition=%wide.region_5.6_spmd.clone, body=%wide.region_4.5_spmd.clone.sunk | while | flops 330284 | bytes 792973 | solution.py:37
  323.6 1.1 fusion.172
  325.5 1.1 fusion.172
  327.4 1.1 fusion.172
  329.7 2.2 fusion.149
  331.9 7.4 %while.13 = (s32[]{:T(128)}, f32[4,128,128]{2,1,0:T(8,128)S(1)}, f32[4,128]{1,0:T(4,128)S(1)}, f32[4]{0:T(128)S(1)}, f32[4]{0:T(128)S(1)}, /*index=5*/s32[]{:T(1...) while((s32[]{:T(128)}, f32[4,128,128]{2,1,0:T(8,128)S(1)}, ...), condition=%wide.region_12.13_spmd.clone, body=%wide.region_11.12_spmd.clone.sunk | while | flops 330288 | bytes 793035 | solution.py:37
  332.6 1.1 fusion.174
  334.5 1.1 fusion.174
  338.2 1.1 fusion.174
  341.2 1.2 fusion.27
  342.5 5.1 rev.26
  347.9 1.7 multiply_reduce_fusion
  349.6 48.5 %all-gather.31.cloned.1.call-done = bf16[2048,1024]{1,0:T(8,128)(2,1)} async-done(((bf16[512,1024]{1,0:T(8,128)(2,1)}), bf16[2048,1024]{1,0:T(8,128)(2,1)}) %all-gather.31.cloned.1.call-update) | async-done | bytes 4194320 | tf_op jit(solution)/shard_map/all_gather | solution.py:220
  398.1 3.5 convolution_convert_fusion
  401.8 1.3 collective-permute-start.2
  403.1 1.3 collective-permute-start.3
  404.5 4.2 collective-permute-done.3
  408.9 70.0 %all-gather.35.cloned.1.call-done = bf16[2048,1024]{1,0:T(8,128)(2,1)} async-done(((bf16[512,1024]{1,0:T(8,128)(2,1)}), bf16[2048,1024]{1,0:T(8,128)(2,1)}) %all-gather.35.cloned.1.call-update) | async-done | bytes 4194320 | tf_op jit(solution)/shard_map/all_gather | solution.py:222
  479.1 5.3 fusion.89
  484.4 40.1 %all-gather.27.cloned.1.call-done = bf16[2048,512]{1,0:T(8,128)(2,1)} async-done(((bf16[512,512]{1,0:T(8,128)(2,1)}), bf16[2048,512]{1,0:T(8,128)(2,1)}) %all-gather.27.cloned.1.call-update) | async-done | bytes 2097168 | tf_op jit(solution)/shard_map/all_gather | solution.py:221
  524.5 3.4 fusion.16
  527.9 7.3 %reduce-scatter.2.cloned.1.call-done = bf16[128,2048]{1,0:T(8,128)(2,1)} async-done(((bf16[256,2048]{1,0:T(8,128)(2,1)}), bf16[128,2048]{1,0:T(8,128)(2,1)}) %reduce-scatter.2.cloned.1.call-update) | async-done | bytes 524304 | tf_op jit(solution)/shard_map/reduce_scatter | solution.py:324
  (236 shorter events, 30.8 us)
Async XLA Ops:
  6.5 26.3 %copy-start.5 = (bf16[128,512]{1,0:T(8,128)(2,1)S(1)}, bf16[128,512]{1,0:T(8,128)(2,1)}, u32[]{:S(2)}) copy-start(bf16[128,512]{1,0:T(8,128)(2,1)} %param.21) | copy-start | bytes 393220
  6.5 36.1 %copy-start.8 = (bf16[4,4,2048]{2,1,0:T(4,128)(2,1)S(1)}, bf16[4,4,2048]{2,1,0:T(4,128)(2,1)}, u32[]{:S(2)}) copy-start(bf16[4,4,2048]{2,1,0:T(4,128)(2,1)} %param.25) | copy-start | bytes 196612
  6.5 36.2 %copy-start.30 = (f32[4,4]{1,0:T(4,128)S(1)}, f32[4,4]{1,0:T(4,128)}, u32[]{:S(2)}) copy-start(f32[4,4]{1,0:T(4,128)} %param.26) | copy-start | bytes 196
  6.5 36.3 %copy-start = (bf16[1,256,2048]{2,1,0:T(8,128)(2,1)S(1)}, bf16[1,256,2048]{2,1,0:T(8,128)(2,1)}, u32[]{:S(2)}) copy-start(bf16[1,256,2048]{2,1,0:T(8,128)(2,1)} %param.19) | copy-start | bytes 3145732
  6.5 59.4 %all-gather.23.cloned.1.call-start = ((), (), s32[]{:S(2)}) async-start(), calls=%async_computation.2 | async-start | bytes 2621440 | tf_op jit(solution)/shard_map/all_gather | solution.py:217
  19.9 23.2 %copy-start.37 = (f32[2048]{0:T(1024)S(1)}, f32[2048]{0:T(1024)}, u32[]{:S(2)}) copy-start(f32[2048]{0:T(1024)} %param.20) | copy-start | bytes 24580
  19.9 92.1 %all-gather.21.cloned.1.call-start = ((), (), s32[]{:S(2)}) async-start(), calls=%async_computation.1 | async-start | bytes 2621440 | tf_op jit(solution)/shard_map/all_gather | solution.py:218
  31.4 107.9 %all-gather.29.cloned.1.call-start = ((), (), s32[]{:S(2)}) async-start(), calls=%async_computation.5 | async-start | bytes 1310720 | tf_op jit(solution)/shard_map/all_gather | solution.py:211
  32.2 135.4 %all-gather.33.cloned.1.call-start = ((), (), s32[]{:S(2)}) async-start(), calls=%async_computation.7 | async-start | bytes 1310720 | tf_op jit(solution)/shard_map/all_gather | solution.py:213
  32.8 282.0 %all-gather.25.cloned.1.call-start = ((), (), s32[]{:S(2)}) async-start(), calls=%async_computation.3 | async-start | bytes 2621440 | tf_op jit(solution)/shard_map/all_gather | solution.py:216
  42.6 278.4 %all-gather.37.cloned.1.call-start = ((), (), s32[]{:S(2)}) async-start(), calls=%async_computation.10 | async-start | bytes 1310720 | tf_op jit(solution)/shard_map/all_gather | solution.py:26
  43.1 68.9 %copy-start.32 = (f32[256]{0:T(256)}, f32[256]{0:T(256)S(1)}, u32[]{:S(2)}) copy-start(f32[256]{0:T(256)S(1)} %add_rsqrt_fusion.1) | copy-start | bytes 3076
  68.3 99.3 %copy-start.4 = (bf16[32,4,8,128]{3,2,1,0:T(8,128)(2,1)}, bf16[32,4,8,128]{3,2,1,0:T(8,128)(2,1)S(1)}, u32[]{:S(2)}) copy-start(bf16[32,4,8,128]{3,2,1,0:T(8,128)(2,1)S(1)} %fusion.51) | copy-start | bytes 786436
  116.3 215.6 %all-gather.39.cloned.1.call-start = ((), (), s32[]{:S(2)}) async-start(), calls=%async_computation.11 | async-start | bytes 1310720 | tf_op jit(solution)/shard_map/all_gather | solution.py:26
  118.9 48.7 %copy-start.6 = (bf16[128,512]{1,0:T(8,128)(2,1)S(1)}, bf16[128,512]{1,0:T(8,128)(2,1)}, u32[]{:S(2)}) copy-start(bf16[128,512]{1,0:T(8,128)(2,1)} %param.24) | copy-start | bytes 393220
  119.3 61.8 %copy-start.7 = (bf16[128,512]{1,0:T(8,128)(2,1)S(1)}, bf16[128,512]{1,0:T(8,128)(2,1)}, u32[]{:S(2)}) copy-start(bf16[128,512]{1,0:T(8,128)(2,1)} %param.32) | copy-start | bytes 393220
  121.5 276.6 %all-gather.31.cloned.1.call-start = ((), (), s32[]{:S(2)}) async-start(), calls=%async_computation.6 | async-start | bytes 5242880 | tf_op jit(solution)/shard_map/all_gather | solution.py:220
  139.3 339.6 %all-gather.35.cloned.1.call-start = ((), (), s32[]{:S(2)}) async-start(), calls=%async_computation.8 | async-start | bytes 5242880 | tf_op jit(solution)/shard_map/all_gather | solution.py:222
  167.5 50.3 %copy-start.41 = (u32[32]{0:T(128)S(1)}, u32[32]{0:T(128)}, u32[]{:S(2)}) copy-start(u32[32]{0:T(128)} %constant.237) | copy-start | bytes 388
  167.6 356.9 %all-gather.27.cloned.1.call-start = ((), (), s32[]{:S(2)}) async-start(), calls=%async_computation.4 | async-start | bytes 2621440 | tf_op jit(solution)/shard_map/all_gather | solution.py:221
  177.7 34.8 %collective-permute-start = (bf16[512,512]{1,0:T(8,128)(2,1)S(1)}, bf16[512,512]{1,0:T(8,128)(2,1)S(1)}, u32[]{:S(2)}, u32[]{:S(2)}) collective-permute-start(bf16[512,512]{1,0:T(8,128)(2,1)S(1)} %all_gather.101), channel_id=1, source_target_pairs={{0,24},{8,0},{16,8},{24,16},{1,25},{9,1},{17,9},{25,17},{2,26},{10... | collective-permute-start | bytes 1572872 | tf_op jit(solution)/shard_map/ppermute | solution.py:17
  191.5 343.7 %reduce-scatter.2.cloned.1.call-start = ((), (), s32[]{:S(2)}) async-start(), calls=%async_computation.9 | async-start | bytes 1572864 | tf_op jit(solution)/shard_map/reduce_scatter | solution.py:324
  213.6 59.5 %collective-permute-start.1 = (bf16[1024,512]{1,0:T(8,128)(2,1)}, bf16[1024,512]{1,0:T(8,128)(2,1)S(1)}, u32[]{:S(2)}, u32[]{:S(2)}) collective-permute-start(bf16[1024,512]{1,0:T(8,128)(2,1)} %pad_maximum_fusion), channel_id=1, source_target_pairs={{0,16},{8,24},{16,0},{24,8},{1,17},{9,25},{17,1},{25,9},{2,18},{10... | collective-permute-start | bytes 3145736 | tf_op jit(solution)/shard_map/ppermute | solution.py:17
  274.4 40.3 %copy-start.2 = (bf16[1,256,2048]{2,1,0:T(8,128)(2,1)S(1)}, bf16[1,256,2048]{2,1,0:T(8,128)(2,1)}, u32[]{:S(2)}) copy-start(bf16[1,256,2048]{2,1,0:T(8,128)(2,1)} %param.19) | copy-start | bytes 3145732
  347.6 50.5 %copy-start.34 = (f32[256]{0:T(256)S(1)}, f32[256]{0:T(256)}, u32[]{:S(2)}) copy-start(f32[256]{0:T(256)} %copy-done.32) | copy-start | bytes 3076
  347.6 50.5 %copy-start.39 = (f32[2048]{0:T(1024)S(1)}, f32[2048]{0:T(1024)}, u32[]{:S(2)}) copy-start(f32[2048]{0:T(1024)} %param.20) | copy-start | bytes 24580
  349.6 54.8 %copy-start.29 = (f32[4,128]{1,0:T(4,128)S(1)}, f32[4,128]{1,0:T(4,128)}, u32[]{:S(2)}) copy-start(f32[4,128]{1,0:T(4,128)} %param.30) | copy-start | bytes 6148
  401.6 77.3 %copy-start.11 = (s32[1024]{0:T(1024)S(1)}, s32[1024]{0:T(1024)}, u32[]{:S(2)}) copy-start(s32[1024]{0:T(1024)} %get-tuple-element.635) | copy-start | bytes 12292
  401.6 77.3 %copy-start.12 = (s32[1024]{0:T(1024)S(1)}, s32[1024]{0:T(1024)}, u32[]{:S(2)}) copy-start(s32[1024]{0:T(1024)} %get-tuple-element.636) | copy-start | bytes 12292
  401.6 77.3 %copy-start.13 = (f32[1024]{0:T(1024)S(1)}, f32[1024]{0:T(1024)}, u32[]{:S(2)}) copy-start(f32[1024]{0:T(1024)} %get-tuple-element.637) | copy-start | bytes 12292
  401.6 77.3 %copy-start.14 = (f32[1024]{0:T(1024)S(1)}, f32[1024]{0:T(1024)}, u32[]{:S(2)}) copy-start(f32[1024]{0:T(1024)} %get-tuple-element.638) | copy-start | bytes 12292
  401.6 77.3 %copy-start.15 = (f32[1024]{0:T(1024)S(1)}, f32[1024]{0:T(1024)}, u32[]{:S(2)}) copy-start(f32[1024]{0:T(1024)} %get-tuple-element.639) | copy-start | bytes 12292
  401.6 77.3 %copy-start.16 = (f32[1024]{0:T(1024)S(1)}, f32[1024]{0:T(1024)}, u32[]{:S(2)}) copy-start(f32[1024]{0:T(1024)} %get-tuple-element.640) | copy-start | bytes 12292
  401.6 77.3 %copy-start.17 = (f32[1024]{0:T(1024)S(1)}, f32[1024]{0:T(1024)}, u32[]{:S(2)}) copy-start(f32[1024]{0:T(1024)} %get-tuple-element.641) | copy-start | bytes 12292
  401.7 77.3 %copy-start.18 = (f32[1024]{0:T(1024)S(1)}, f32[1024]{0:T(1024)}, u32[]{:S(2)}) copy-start(f32[1024]{0:T(1024)} %get-tuple-element.642) | copy-start | bytes 12292
  401.7 77.3 %copy-start.19 = (f32[1024]{0:T(1024)S(1)}, f32[1024]{0:T(1024)}, u32[]{:S(2)}) copy-start(f32[1024]{0:T(1024)} %get-tuple-element.643) | copy-start | bytes 12292
  401.7 77.3 %copy-start.20 = (f32[1024]{0:T(1024)S(1)}, f32[1024]{0:T(1024)}, u32[]{:S(2)}) copy-start(f32[1024]{0:T(1024)} %get-tuple-element.644) | copy-start | bytes 12292
  401.7 77.3 %copy-start.21 = (f32[1024]{0:T(1024)S(1)}, f32[1024]{0:T(1024)}, u32[]{:S(2)}) copy-start(f32[1024]{0:T(1024)} %get-tuple-element.645) | copy-start | bytes 12292
  401.7 77.3 %copy-start.22 = (f32[1024]{0:T(1024)S(1)}, f32[1024]{0:T(1024)}, u32[]{:S(2)}) copy-start(f32[1024]{0:T(1024)} %get-tuple-element.646) | copy-start | bytes 12292
  401.7 77.3 %copy-start.23 = (f32[1024]{0:T(1024)S(1)}, f32[1024]{0:T(1024)}, u32[]{:S(2)}) copy-start(f32[1024]{0:T(1024)} %get-tuple-element.647) | copy-start | bytes 12292
  401.7 77.3 %copy-start.24 = (f32[1024]{0:T(1024)S(1)}, f32[1024]{0:T(1024)}, u32[]{:S(2)}) copy-start(f32[1024]{0:T(1024)} %get-tuple-element.648) | copy-start | bytes 12292
  401.7 77.3 %copy-start.25 = (f32[1024]{0:T(1024)S(1)}, f32[1024]{0:T(1024)}, u32[]{:S(2)}) copy-start(f32[1024]{0:T(1024)} %get-tuple-element.649) | copy-start | bytes 12292
  401.7 77.3 %copy-start.26 = (f32[1024]{0:T(1024)S(1)}, f32[1024]{0:T(1024)}, u32[]{:S(2)}) copy-start(f32[1024]{0:T(1024)} %get-tuple-element.650) | copy-start | bytes 12292
  401.7 77.3 %copy-start.27 = (f32[1024]{0:T(1024)S(1)}, f32[1024]{0:T(1024)}, u32[]{:S(2)}) copy-start(f32[1024]{0:T(1024)} %get-tuple-element.651) | copy-start | bytes 12292
  401.8 77.3 %copy-start.28 = (f32[1024]{0:T(1024)S(1)}, f32[1024]{0:T(1024)}, u32[]{:S(2)}) copy-start(f32[1024]{0:T(1024)} %get-tuple-element.652) | copy-start | bytes 12292
  401.8 77.3 %copy-start.40 = (s32[256]{0:T(256)S(1)}, s32[256]{0:T(256)}, u32[]{:S(2)}) copy-start(s32[256]{0:T(256)} %iota_add_fusion.1) | copy-start | bytes 3076
  401.8 2.8 collective-permute-start.2
  403.1 5.7 %collective-permute-start.3 = (bf16[8,1024]{1,0:T(8,128)(2,1)S(1)}, bf16[8,1024]{1,0:T(8,128)(2,1)S(1)}, u32[]{:S(2)}, u32[]{:S(2)}) collective-permute-start(bf16[8,1024]{1,0:T(8,128)(2,1)S(1)} %get-tuple-element.621), channel_id=1, source_target_pairs={{8,0},{16,8},{24,16},{9,1},{17,9},{25,17},{10,2},{18,10},{26,18},{... | collective-permute-start | bytes 49160 | tf_op jit(solution)/shard_map/ppermute | solution.py:48
  (10 other events, 57.6 us)
Sparse Core Ops, SparseCore 0:
  20.0 45.9 all-gather.22
  67.6 44.4 all-gather.20
  113.9 25.3 all-gather.28
  141.0 26.4 all-gather.32
  168.9 83.6 all-gather.24
  254.1 31.9 all-gather.36
  287.6 28.6 all-gather.38
  317.9 80.1 all-gather.30
  399.7 79.1 all-gather.34
  480.3 44.1 all-gather.26
  528.0 7.1 reduce-scatter.1
